TPU v7x, 32 devices: a whole 2x2x4 slice. The times are simulated.
32 devices in a mesh: sp: 8 (over z, y), tp: 4 (over x, core).
Axes of the slice: x: 2, y: 2, z: 4, core: 2. Of those that a mesh axis runs over, the one named last changes fastest.
Arguments:
- hidden: bfloat16 [1024, 2048], P('sp'), may hold values from -6 to 6
- value_weight: bfloat16 [2048, 4096], P(None, 'tp'), may hold values from -0.125 to 0.125
- key_vecs: bfloat16 [1024, 8, 128], P('sp', 'tp'), may hold values from -0.29882812 to 0.29882812
- queries: bfloat16 [1024, 8, 128], P('sp', 'tp'), may hold values from -0.29882812 to 0.29882812
- decay_pre: float32 [1024, 64], P('sp', 'tp'), may hold values from -4 to 4
- decay_rate: float32 [64], P('tp'), may hold values from 5.859375e-05 to 0.0036132813
- cotangent: bfloat16 [1024, 64, 64], P('sp', 'tp'), may hold values from -1.1953125 to 1.1953125
Outputs:
- grad_keys: bfloat16 [1024, 8, 128], P('sp', 'tp')
- grad_queries: bfloat16 [1024, 8, 128], P('sp', 'tp')
- grad_decay: float32 [1024, 64], P('sp', 'tp')
- grad_hidden: bfloat16 [1024, 2048], P(('sp', 'tp'))
- grad_weight: float32 [2048, 4096], P('sp', 'tp')
All inputs are finite; a program needn't handle non-finite values.
Results may differ from a plain program's by a relative error of at most 0.003.
Values sent between devices are 32-bit elements.
A program may use at most 64 MiB of HBM per device.

v0:
```python
import jax
import jax.numpy as jnp
from jax import lax
from jax.sharding import PartitionSpec as P

highest = lax.Precision.HIGHEST


def over_all(array, axis, dim, update, carry):
    whole = jax.tree.map(lambda part: lax.all_gather(part, axis, axis=dim, tiled=True), array)
    return update(carry, whole, jnp.int32(0))


def summed_rows(product, span, axis):
    everything = product(jnp.int32(0), lax.axis_size(axis) * span)
    own = lax.psum_scatter(everything, axis, scatter_dimension=0, tiled=True)
    return own


def local_mixer(values_f, keys_f, queries_f, decay_pre, decay_rate, state_in):
    heads_here = values_f.shape[1]
    per_group = heads_here // keys_f.shape[1]
    key_heads = jnp.repeat(keys_f, per_group, axis=1)
    query_heads = jnp.repeat(queries_f, per_group, axis=1)
    log_decay = -decay_rate[None, :] * jax.nn.softplus(decay_pre)
    cumulative = jnp.cumsum(log_decay, axis=0)
    length = values_f.shape[0]
    causal = jnp.tril(jnp.ones((length, length), dtype=bool))[None]
    across = cumulative.T[:, :, None] - cumulative.T[:, None, :]
    damping = jnp.where(causal, jnp.exp(jnp.where(causal, across, 0.0)), 0.0)
    scores = jnp.einsum("thn,shn->hts", query_heads, key_heads, precision=highest)
    outputs = jnp.einsum("hts,shp->thp", scores * damping, values_f, precision=highest)
    carried = jnp.einsum("thn,hpn->thp", query_heads, state_in, precision=highest)
    outputs = outputs + jnp.exp(cumulative)[:, :, None] * carried
    to_end = jnp.exp(cumulative[-1][None, :] - cumulative)
    state_out = jnp.exp(cumulative[-1])[:, None, None] * state_in + jnp.einsum(
        "sh,shp,shn->hpn", to_end, values_f, key_heads, precision=highest
    )
    return (outputs, state_out)


def per_device(hidden, value_weight, key_vecs, queries, decay_pre, decay_rate, cotangent):
    length = hidden.shape[0]
    heads_here = decay_rate.shape[0]
    head_width = cotangent.shape[2]
    values = jnp.dot(hidden, value_weight, preferred_element_type=jnp.float32).astype(jnp.bfloat16)
    values_f = values.reshape(length, heads_here, head_width).astype(jnp.float32)
    keys_f = key_vecs.astype(jnp.float32)
    queries_f = queries.astype(jnp.float32)
    grads_out = cotangent.astype(jnp.float32)
    per_group = heads_here // keys_f.shape[1]
    key_heads = jnp.repeat(keys_f, per_group, axis=1)
    query_heads = jnp.repeat(queries_f, per_group, axis=1)
    cumulative = jnp.cumsum(-decay_rate[None, :] * jax.nn.softplus(decay_pre), axis=0)
    decay_total = cumulative[-1]
    to_end = jnp.exp(decay_total[None, :] - cumulative)
    local_state = jnp.einsum("sh,shp,shn->hpn", to_end, values_f, key_heads, precision=highest)
    local_pull = jnp.einsum(
        "th,thp,thn->hpn", jnp.exp(cumulative), grads_out, query_heads, precision=highest
    )
    totals = lax.all_gather(decay_total[None, :], "sp", axis=0, tiled=True)
    running = jnp.cumsum(totals, axis=0)
    position = lax.axis_index("sp")
    own_end = lax.dynamic_slice_in_dim(running, position, 1, 0)[0]
    own_start = own_end - decay_total

    def absorb(sums_now, pieces, start):
        count = pieces[0].shape[0]
        end_logs = lax.dynamic_slice_in_dim(running, start, count, 0)
        starts = end_logs - lax.dynamic_slice_in_dim(totals, start, count, 0)
        index = start + jnp.arange(count, dtype=jnp.int32)
        earlier_mask = (index < position)[:, None]
        later_mask = (index > position)[:, None]
        ahead_w = jnp.where(
            earlier_mask, jnp.exp(jnp.where(earlier_mask, own_start[None, :] - end_logs, 0.0)), 0.0
        )
        behind_w = jnp.where(
            later_mask, jnp.exp(jnp.where(later_mask, starts - own_end[None, :], 0.0)), 0.0
        )
        return (
            sums_now[0] + jnp.einsum("kh,khpn->hpn", ahead_w, pieces[0], precision=highest),
            sums_now[1] + jnp.einsum("kh,khpn->hpn", behind_w, pieces[1], precision=highest),
        )

    empty = jnp.zeros_like(local_state)
    state_in, state_grad = over_all(
        (local_state[None], local_pull[None]), "sp", 0, absorb, (empty, empty)
    )

    def local_part(values_in, keys_in, queries_in, pre_in):
        return local_mixer(values_in, keys_in, queries_in, pre_in, decay_rate, state_in)

    primal, pullback = jax.vjp(local_part, values_f, keys_f, queries_f, decay_pre)
    grad_values, grad_keys, grad_queries, grad_decay = pullback((grads_out, state_grad))
    grad_flat = grad_values.reshape(length, -1).astype(jnp.bfloat16)

    def input_term(start, count):
        rows_now = lax.dynamic_slice_in_dim(grad_flat, start, count, 0)
        return lax.dot_general(
            rows_now, value_weight, (((1,), (1,)), ((), ())), preferred_element_type=jnp.float32
        )

    grad_hidden = summed_rows(input_term, length // lax.axis_size("tp"), "tp").astype(jnp.bfloat16)

    def weight_term(start, count):
        columns = lax.dynamic_slice_in_dim(hidden, start, count, 1)
        return lax.dot_general(
            columns, grad_flat, (((0,), (0,)), ((), ())), preferred_element_type=jnp.float32
        )

    grad_weight = summed_rows(weight_term, hidden.shape[1] // lax.axis_size("sp"), "sp")
    return (
        grad_keys.astype(jnp.bfloat16),
        grad_queries.astype(jnp.bfloat16),
        grad_decay,
        grad_hidden,
        grad_weight,
    )


def solution(mesh):
    return jax.shard_map(
        per_device,
        mesh=mesh,
        in_specs=(
            P("sp", None),
            P(None, "tp"),
            P("sp", "tp", None),
            P("sp", "tp", None),
            P("sp", "tp"),
            P("tp"),
            P("sp", "tp", None),
        ),
        out_specs=(
            P("sp", "tp", None),
            P("sp", "tp", None),
            P("sp", "tp"),
            P(("sp", "tp"), None),
            P("sp", "tp"),
        ),
        check_vma=False,
    )
```

profile of v0, /device:TPU:0, one launch (start us, length us, event | category | flops | bytes accessed | tf_op | source)
XLA Modules:
  0.0 360.7 jit_solution(991508006795061754)
XLA Ops:
  7.2 0.7 neg.19
  7.9 0.8 copy.114
  8.8 0.2 reduce_window_sum.35
  9.0 0.9 copy.123
  10.0 2.9 fusion.20
  13.0 0.2 slice_reduce_fusion
  13.2 22.4 %all-gather.2 = f32[8,1,16]{2,1,0:T(1,128)S(1)} all-gather(f32[1,1,16]{2,1,0:T(1,128)S(1)} %bitcast.114), channel_id=1, replica_groups=mesh['sp'=8,'tp'=4] {'sp'}, dimensions={0}, use_global_device_ids=true | all-gather | bytes 576 | tf_op jit(solution)/shard_map/all_gather | solution.py:61
  35.7 0.2 reduce_window_sum.36
  35.9 2.9 convolution_convert_fusion
  38.8 0.2 copy.125
  39.0 0.2 subtract_reduce_fusion
  39.2 0.7 exponential_select_fusion
  39.9 0.4 convolution_bitcast_fusion.1
  40.3 0.1 broadcast_in_dim.86
  40.4 0.9 copy-done.1
  41.3 3.9 %fusion.44 = (f32[16,128]{1,0:T(8,128)S(1)}, f32[16,128]{1,0:T(8,128)}, f32[16,128,128]{1,2,0:T(8,128)}) fusion(f32[16,128]{1,0:T(8,128)S(1)} %copy.126, f32[16,128,128]{1,2,0:T(8,128)S(1)} %convolution_bitcast_fusion.1, pred[128,128]{0,1:T(8,128)(4,1)S(1)} %iota_compare_fusion, f32[128,16,128]{2,0,1:T(8,128)S(1)} %bitcast.90, f32[128,16,128]{2,0,1:T(8,128)S(1)} %bitcast.93), kind=kOutput, calls=%fused_computation.55 | convolution fusion | flops 404746240 | bytes 4235264 | tf_op jit(solution)/shard_map/jvp(thn,shn->hts)/dot_general | solution.py:31
  45.2 43.8 %all-gather.6.cloned.1.call-done = f32[128,64,128]{2,1,0:T(8,128)} async-done(((f32[16,64,128]{2,1,0:T(8,128)}), f32[128,64,128]{2,1,0:T(8,128)}) %all-gather.6.cloned.1.call-update) | async-done | bytes 4194320 | tf_op jit(solution)/shard_map/all_gather | solution.py:10
  89.0 8.3 %fusion.2 = f32[16,1,64,128]{3,1,2,0:T(1,128)S(1)} fusion(f32[8,16,1,1]{0,2,3,1:T(1,128)S(1)} %bitcast.112, f32[8,16,64,128]{3,2,1,0:T(8,128)} %bitcast.106), kind=kOutput, calls=%fused_computation.3 | convolution fusion | flops 12582912 | bytes 4719104 | tf_op jit(solution)/shard_map/kh,khpn->hpn/dot_general | solution.py:82
  97.3 2.1 fusion.24
  99.5 0.7 multiply_reduce_fusion.1
  100.2 1.3 fusion.7
  101.6 0.7 copy-done.8
  102.3 2.7 fusion.52
  105.0 1.9 fusion.21
  107.0 5.4 %convolution_bitcast_fusion = f32[2048,1024]{0,1:T(8,128)} fusion(bf16[128,1024]{0,1:T(8,128)(2,1)} %bitcast.109, bf16[128,2048]{1,0:T(8,128)(2,1)S(1)} %copy-done), kind=kOutput, calls=%fused_computation | convolution fusion | flops 536870912 | bytes 9175040 | tf_op jit(solution)/shard_map/dot_general | solution.py:107
  112.4 0.7 copy-done.12
  113.1 0.6 broadcast_compare_fusion
  113.6 0.8 copy.136
  114.4 1.3 copy.132
  115.8 1.8 convolution_bitcast_fusion.3
  117.6 3.5 bitcast_reduce_fusion.1
  121.1 0.8 copy.140
  121.8 6.1 %reduce-scatter.3.cloned.1.call-done = f32[32,2048]{1,0:T(8,128)} async-done(((f32[128,2048]{1,0:T(8,128)}), f32[32,2048]{1,0:T(8,128)}) %reduce-scatter.3.cloned.1.call-update) | async-done | bytes 262160 | tf_op jit(solution)/shard_map/reduce_scatter | solution.py:16
  128.0 1.6 convert_element_type.33
  129.6 73.7 %all-gather.8.cloned.1.call-done = f32[128,64,128]{2,1,0:T(8,128)} async-done(((f32[16,64,128]{2,1,0:T(8,128)}), f32[128,64,128]{2,1,0:T(8,128)}) %all-gather.8.cloned.1.call-update) | async-done | bytes 4194320 | tf_op jit(solution)/shard_map/all_gather | solution.py:10
  203.2 8.3 %fusion = f32[16,1,64,128]{3,1,2,0:T(1,128)S(1)} fusion(f32[8,16,1,1]{0,2,3,1:T(1,128)} %bitcast.111, f32[8,16,64,128]{3,2,1,0:T(8,128)} %bitcast.107), kind=kOutput, calls=%fused_computation.1 | convolution fusion | flops 12582912 | bytes 4719104 | tf_op jit(solution)/shard_map/kh,khpn->hpn/dot_general | solution.py:81
  211.5 0.7 multiply_reduce_fusion
  212.2 1.3 copy.131
  213.6 2.0 fusion.22
  215.6 3.4 bitcast_reduce_fusion
  219.1 0.7 copy.141
  219.8 2.1 fusion.8
  222.1 0.1 copy.134
  222.2 1.1 reduce_window_sum.37
  223.3 0.6 fusion.47
  223.9 0.7 copy.142
  224.6 127.1 %reduce-scatter.5.cloned.1.call-done = f32[256,1024]{0,1:T(8,128)} async-done(((f32[2048,1024]{0,1:T(8,128)}), f32[256,1024]{0,1:T(8,128)}) %reduce-scatter.5.cloned.1.call-update) | async-done | bytes 1048592 | tf_op jit(solution)/shard_map/reduce_scatter | solution.py:16
  351.7 2.5 copy.143
  (48 shorter events, 0.8 us)
Async XLA Ops:
  7.2 28.7 %copy-start = (bf16[128,2048]{1,0:T(8,128)(2,1)S(1)}, bf16[128,2048]{1,0:T(8,128)(2,1)}, u32[]{:S(2)}) copy-start(bf16[128,2048]{1,0:T(8,128)(2,1)} %param.7) | copy-start | bytes 1572868
  7.2 28.7 %copy-start.10 = (bf16[128,2,128]{2,1,0:T(2,128)(2,1)S(1)}, bf16[128,2,128]{2,1,0:T(2,128)(2,1)}, u32[]{:S(2)}) copy-start(bf16[128,2,128]{2,1,0:T(2,128)(2,1)} %param.9) | copy-start | bytes 196612
  7.2 81.8 %all-gather.6.cloned.1.call-start = ((), (), s32[]{:S(2)}) async-start(), calls=%async_computation.4 | async-start | bytes 4718592 | tf_op jit(solution)/shard_map/all_gather | solution.py:10
  7.9 30.9 %copy-start.15 = (f32[16]{0:T(128)}, f32[16]{0:T(128)S(1)}, u32[]{:S(2)}) copy-start(f32[16]{0:T(128)S(1)} %neg.19) | copy-start | bytes 196
  10.0 29.9 %copy-start.5 = (bf16[128,16,64]{0,2,1:T(8,128)(2,1)S(1)}, bf16[128,16,64]{0,2,1:T(8,128)(2,1)}, u32[]{:S(2)}) copy-start(bf16[128,16,64]{0,2,1:T(8,128)(2,1)} %param.13) | copy-start | bytes 786436
  12.9 115.0 %reduce-scatter.3.cloned.1.call-start = ((), (), s32[]{:S(2)}) async-start(), calls=%async_computation.2 | async-start | bytes 1310720 | tf_op jit(solution)/shard_map/reduce_scatter | solution.py:16
  40.3 1.0 copy-start.1
  89.0 11.2 %copy-start.6 = (bf16[128,16,64]{0,2,1:T(8,128)(2,1)S(1)}, bf16[128,16,64]{0,2,1:T(8,128)(2,1)}, u32[]{:S(2)}) copy-start(bf16[128,16,64]{0,2,1:T(8,128)(2,1)} %param.13) | copy-start | bytes 786436
  89.0 11.2 %copy-start.9 = (f32[16,128,128]{1,2,0:T(8,128)S(1)}, f32[16,128,128]{1,2,0:T(8,128)}, u32[]{:S(2)}) copy-start(f32[16,128,128]{1,2,0:T(8,128)} %get-tuple-element.40) | copy-start | bytes 3145732
  89.0 13.3 %copy-start.2 = (bf16[2048,1024]{1,0:T(8,128)(2,1)S(1)}, bf16[2048,1024]{1,0:T(8,128)(2,1)}, u32[]{:S(2)}) copy-start(bf16[2048,1024]{1,0:T(8,128)(2,1)} %param.8) | copy-start | bytes 12582916
  97.3 18.4 %copy-start.3 = (f32[16,1,64,128]{3,1,2,0:T(1,128)}, f32[16,1,64,128]{3,1,2,0:T(1,128)S(1)}, u32[]{:S(2)}) copy-start(f32[16,1,64,128]{3,1,2,0:T(1,128)S(1)} %fusion.2) | copy-start | bytes 1572868
  101.5 0.7 copy-start.8
  104.9 98.3 %all-gather.8.cloned.1.call-start = ((), (), s32[]{:S(2)}) async-start(), calls=%async_computation.5 | async-start | bytes 4718592 | tf_op jit(solution)/shard_map/all_gather | solution.py:10
  106.9 244.8 %reduce-scatter.5.cloned.1.call-start = ((), (), s32[]{:S(2)}) async-start(), calls=%async_computation.3 | async-start | bytes 9437184 | tf_op jit(solution)/shard_map/reduce_scatter | solution.py:16
  112.4 0.7 copy-start.12
  117.6 96.0 %copy-start.7 = (bf16[128,16,64]{0,2,1:T(8,128)(2,1)S(1)}, bf16[128,16,64]{0,2,1:T(8,128)(2,1)}, u32[]{:S(2)}) copy-start(bf16[128,16,64]{0,2,1:T(8,128)(2,1)} %param.13) | copy-start | bytes 786436
  203.2 8.3 %copy-start.4 = (f32[16,1,64,128]{3,1,2,0:T(1,128)S(1)}, f32[16,1,64,128]{3,1,2,0:T(1,128)}, u32[]{:S(2)}) copy-start(f32[16,1,64,128]{3,1,2,0:T(1,128)} %copy-done.3) | copy-start | bytes 1572868
  213.6 8.3 %copy-start.14 = (f32[1,16]{0,1:T(8,128)S(1)}, f32[1,16]{0,1:T(8,128)}, u32[]{:S(2)}) copy-start(f32[1,16]{0,1:T(8,128)} %copy.131) | copy-start | bytes 196
  213.6 8.4 %copy-start.11 = (f32[16,128]{1,0:T(8,128)S(1)}, f32[16,128]{1,0:T(8,128)}, u32[]{:S(2)}) copy-start(f32[16,128]{1,0:T(8,128)} %get-tuple-element.31) | copy-start | bytes 24580
  213.6 8.4 %copy-start.13 = (f32[1,16]{0,1:T(8,128)S(1)}, f32[1,16]{0,1:T(8,128)}, u32[]{:S(2)}) copy-start(f32[1,16]{0,1:T(8,128)} %copy.132) | copy-start | bytes 196
Sparse Core Ops, SparseCore 0:
  13.1 75.8 all-gather.5
  105.1 22.8 reduce-scatter.2
  130.1 73.1 all-gather.7
  206.7 144.9 reduce-scatter.4
where the time goes:
time: 361 us
  waiting for transfers between devices  251 us (70%)
  matrix products  53 us (15%)
  blocking collectives  22.4 us (6%)
  between operations  14 us (4%)
  local copies, waits for them, and re-layouts  12.9 us (4%)
  other arithmetic  7.52 us (2%)
    reduce_scatter x2, waiting for transfers between devices, summed_rows(): own = lax.psum_scatter(everything, axis, scatter_dimension=0, tiled=True)  133 us
    all_gather x2, waiting for transfers between devices, over_all(): lax.all_gather(part, axis, axis=dim, tiled=True)  117 us
    all_gather x1, blocking collectives, per_device(): totals = lax.all_gather(decay_total[None, :], 'sp', axis=0, tiled=True)  22.4 us
    dot_general x3, matrix products, local_mixer(): jnp.einsum('thn,shn->hts', query_heads, key_heads, precision=highest)  10.8 us
    dot_general x1, matrix products, absorb(): jnp.einsum('kh,khpn->hpn', behind_w, pieces[1], precision=highest)  8.34 us
    dot_general x1, matrix products, absorb(): jnp.einsum('kh,khpn->hpn', ahead_w, pieces[0], precision=highest)  8.27 us
    unnamed x38, local copies, waits for them, and re-layouts  7.82 us
  transfers between devices with their start and end apart: 4, of which 4 were waited for; matrix products, arithmetic and copies ran while one was open for 13% of the time, Pallas kernels for 0%

commit v1 on v0

v1 whole, which is shorter than its diff:
```python
import functools

import jax
import jax.numpy as jnp
from jax import lax
from jax.experimental import pallas as pl
from jax.experimental.pallas import tpu as pltpu
from jax.sharding import PartitionSpec as P

MESH = pl.DeviceIdType.MESH
F32 = jnp.float32
BF16 = jnp.bfloat16


def inner_size(count):
    size = 1
    while size * size * 4 <= count:
        size *= 2
    while count % size:
        size -= 1
    return size


def remote(src, dst, send, recv, axis, index):
    return pltpu.make_async_remote_copy(
        src_ref=src, dst_ref=dst, send_sem=send, recv_sem=recv, device_id={axis: index}, device_id_type=MESH
    )


def scan_kernel(ny, nz, both_ref, dec_ref, hid_ref, out_ref, hcol_ref,
                ybuf, ydec, pin, pout, hid_f, hland,
                ysend, yrecv, dsend, drecv, psend, precv, hsend, hrecv):
    me = lax.axis_index("sp")
    z, y = me // ny, me % ny
    heads = both_ref.shape[0]
    span = hland.shape[2]

    barrier = pltpu.get_barrier_semaphore()
    for dy in range(1, ny):
        pl.semaphore_signal(barrier, inc=1, device_id={"sp": z * ny + (y + dy) % ny}, device_id_type=MESH)
    for dz in range(1, nz):
        pl.semaphore_signal(barrier, inc=1, device_id={"sp": ((z + dz) % nz) * ny + y}, device_id_type=MESH)
    pl.semaphore_wait(barrier, ny - 1 + nz - 1)

    def ycopy(h, dy):
        there = (y + dy) % ny
        return remote(both_ref.at[h], ybuf.at[y, h], ysend.at[there, h], yrecv.at[y, h], "sp", z * ny + there)

    def yarrive(h, there):
        return remote(both_ref.at[h], ybuf.at[there, h], ysend.at[there, h], yrecv.at[there, h], "sp", z * ny + there)

    def dcopy(dy):
        there = (y + dy) % ny
        return remote(dec_ref, ydec.at[y], dsend.at[there], drecv.at[y], "sp", z * ny + there)

    def darrive(dy):
        there = (y + dy) % ny
        return remote(dec_ref, ydec.at[there], dsend.at[there], drecv.at[there], "sp", z * ny + there)

    for dy in range(1, ny):
        dcopy(dy).start()

    def launch(h, carry):
        for dy in range(1, ny):
            ycopy(h, dy).start()
        return carry

    lax.fori_loop(0, heads, launch, 0)

    def hcopy(dz):
        there = (z + dz) % nz
        return remote(
            hid_f.at[:, pl.ds(pl.multiple_of(there * span, 128), span)], hland.at[z],
            hsend.at[there], hrecv.at[z], "sp", there * ny + y,
        )

    def harrive(dz):
        there = (z + dz) % nz
        return remote(
            hid_f.at[:, pl.ds(pl.multiple_of(there * span, 128), span)], hland.at[there],
            hsend.at[there], hrecv.at[there], "sp", there * ny + y,
        )

    hid_f[...] = hid_ref[...].astype(F32)
    for dz in range(1, nz):
        hcopy(dz).start()
    ybuf[y] = both_ref[...]
    ydec[y] = dec_ref[...]
    for dy in range(1, ny):
        darrive(dy).wait_recv()

    @pl.when(z == 0)
    def _():
        pin[0] = jnp.zeros_like(pin[0])

    @pl.when(z == nz - 1)
    def _():
        pin[1] = jnp.zeros_like(pin[1])

    def up(h):
        return remote(pout.at[0, h], pin.at[0, h], psend.at[0, h], precv.at[0, h], "sp", me + ny)

    def down(h):
        return remote(pout.at[1, h], pin.at[1, h], psend.at[1, h], precv.at[1, h], "sp", me - ny)

    def ready(h, first):
        @pl.when(first)
        def _():
            for dy in range(1, ny):
                yarrive(h, (y + dy) % ny).wait_recv()

    def step(t, carry):
        a = t - z
        b = t - (nz - 1 - z)

        @pl.when((a >= 0) & (a < heads))
        def _():
            ready(a, (2 * z <= nz - 1))

            @pl.when(z > 0)
            def _():
                up(a).wait_recv()

            now = pin[0, a]
            for yy in range(ny):
                @pl.when(y == yy)
                def _():
                    out_ref[a, 0] = now

                now = ydec[yy, a] * now + ybuf[yy, a, 0]
            pout[0, a] = now

            @pl.when(z < nz - 1)
            def _():
                up(a).start()

        @pl.when((b >= 0) & (b < heads))
        def _():
            ready(b, (2 * z > nz - 1))

            @pl.when(z < nz - 1)
            def _():
                down(b).wait_recv()

            now = pin[1, b]
            for yy in reversed(range(ny)):
                @pl.when(y == yy)
                def _():
                    out_ref[b, 1] = now

                now = ydec[yy, b] * now + ybuf[yy, b, 1]
            pout[1, b] = now

            @pl.when(z > 0)
            def _():
                down(b).start()

        return carry

    lax.fori_loop(0, heads + nz - 1, step, 0)

    hcol_ref[pl.ds(pl.multiple_of(z * hland.shape[1], 128), hland.shape[1]), :] = (
        hid_f[:, pl.ds(pl.multiple_of(z * span, 128), span)].astype(BF16)
    )
    for dz in range(1, nz):
        there = (z + dz) % nz
        harrive(dz).wait_recv()
        hcol_ref[pl.ds(pl.multiple_of(there * hland.shape[1], 128), hland.shape[1]), :] = hland[there].astype(BF16)
    for dz in range(1, nz):
        hcopy(dz).wait_send()
    for dy in range(1, ny):
        dcopy(dy).wait_send()

    def drain(h, carry):
        for dy in range(1, ny):
            ycopy(h, dy).wait_send()

        @pl.when(z < nz - 1)
        def _():
            up(h).wait_send()

        @pl.when(z > 0)
        def _():
            down(h).wait_send()

        return carry

    lax.fori_loop(0, heads, drain, 0)


def grads_kernel(ny, nz, ntp, width, gv_ref, hct_ref, ghp_ref, gw_ref, gh_ref,
                 gath, part, land, ghland,
                 upsend, dnsend, grecv, ysend, yrecv, hsend, hrecv):
    me = lax.axis_index("sp")
    mine = lax.axis_index("tp")
    z, y = me // ny, me % ny
    rows = gw_ref.shape[0]
    chunks = gv_ref.shape[1] // width
    length = gv_ref.shape[0]
    own_rows = gh_ref.shape[0]

    barrier = pltpu.get_barrier_semaphore()
    for dy in range(1, ny):
        pl.semaphore_signal(barrier, inc=1, device_id={"sp": z * ny + (y + dy) % ny}, device_id_type=MESH)
    for dz in (1, nz - 1):
        pl.semaphore_signal(barrier, inc=1, device_id={"sp": ((z + dz) % nz) * ny + y}, device_id_type=MESH)
    for dt in range(1, ntp):
        pl.semaphore_signal(barrier, inc=1, device_id={"tp": (mine + dt) % ntp}, device_id_type=MESH)
    pl.semaphore_wait(barrier, ny - 1 + 2 + ntp - 1)

    def cols(c):
        return pl.ds(pl.multiple_of(c * width, 128), width)

    def up(b, c):
        return remote(gath.at[b, c], gath.at[b, c], upsend.at[b, c], grecv.at[b, c], "sp", me + ny)

    def down(b, c):
        return remote(gath.at[b, c], gath.at[b, c], dnsend.at[b, c], grecv.at[b, c], "sp", me - ny)

    def launch(c, carry):
        gath[z, c] = gv_ref[:, cols(c)]

        @pl.when(z < nz - 1)
        def _():
            up(z, c).start()

        @pl.when(z > 0)
        def _():
            down(z, c).start()

        return carry

    lax.fori_loop(0, chunks, launch, 0)

    def hcopy(dt):
        there = (mine + dt) % ntp
        return remote(
            ghp_ref.at[pl.ds(pl.multiple_of(there * own_rows, 8), own_rows), :], ghland.at[mine],
            hsend.at[there], hrecv.at[mine], "tp", there,
        )

    def harrive(dt):
        there = (mine + dt) % ntp
        return remote(
            ghp_ref.at[pl.ds(pl.multiple_of(there * own_rows, 8), own_rows), :], ghland.at[there],
            hsend.at[there], hrecv.at[there], "tp", there,
        )

    for dt in range(1, ntp):
        hcopy(dt).start()

    def ycopy(c, there):
        return remote(
            part.at[there, c], land.at[y, c], ysend.at[there, c], yrecv.at[y, c], "sp", z * ny + there
        )

    def yarrive(c, there):
        return remote(
            part.at[there, c], land.at[there, c], ysend.at[there, c], yrecv.at[there, c], "sp", z * ny + there
        )

    def work(c, carry):
        for d in range(1, nz):
            low, high = z - d, z + d

            @pl.when(low >= 0)
            def _():
                down(jnp.maximum(low, 0), c).wait_recv()

                @pl.when(z < nz - 1)
                def _():
                    up(jnp.maximum(low, 0), c).start()

            @pl.when(high < nz)
            def _():
                up(jnp.minimum(high, nz - 1), c).wait_recv()

                @pl.when(z > 0)
                def _():
                    down(jnp.minimum(high, nz - 1), c).start()

        block = gath[:, c].reshape(nz * length, width).astype(BF16)
        for dy in range(1, ny):
            there = (y + dy) % ny
            part[there, c] = jnp.dot(
                hct_ref[pl.ds(pl.multiple_of(there * rows, 8), rows), :], block, preferred_element_type=F32
            )
            ycopy(c, there).start()
        gw_ref[:, cols(c)] = jnp.dot(
            hct_ref[pl.ds(pl.multiple_of(y * rows, 8), rows), :], block, preferred_element_type=F32
        )
        return carry

    lax.fori_loop(0, chunks, work, 0)

    total = ghp_ref[pl.ds(pl.multiple_of(mine * own_rows, 8), own_rows), :]
    for dt in range(1, ntp):
        harrive(dt).wait_recv()
        total = total + ghland[(mine + dt) % ntp]
    gh_ref[...] = total.astype(gh_ref.dtype)

    def collect(c, carry):
        for dy in range(1, ny):
            there = (y + dy) % ny
            yarrive(c, there).wait_recv()
            gw_ref[:, cols(c)] += land[there, c]
        return carry

    lax.fori_loop(0, chunks, collect, 0)

    def drain(c, carry):
        for dy in range(1, ny):
            ycopy(c, (y + dy) % ny).wait_send()
        for b in range(nz):
            @pl.when((b <= z) & (z < nz - 1))
            def _():
                up(b, c).wait_send()

            @pl.when((b >= z) & (z > 0))
            def _():
                down(b, c).wait_send()

        return carry

    lax.fori_loop(0, chunks, drain, 0)
    for dt in range(1, ntp):
        hcopy(dt).wait_send()


VM = pl.BlockSpec(memory_space=pltpu.VMEM)
LIMIT = 48 * 1024 * 1024


def split(x):
    hi = lax.reduce_precision(x, 8, 7)
    return hi.astype(BF16), (x - hi).astype(BF16)


def two_pass(spec, x, y):
    hi, lo = split(x)
    return jnp.einsum(spec, hi, y, preferred_element_type=F32) + jnp.einsum(spec, lo, y, preferred_element_type=F32)


def per_device(sp, tp, hidden, value_weight, key_vecs, queries, decay_pre, decay_rate, cotangent):
    length = hidden.shape[0]
    heads = decay_rate.shape[0]
    head_width = cotangent.shape[2]
    groups = key_vecs.shape[1]
    state = key_vecs.shape[2]
    per = heads // groups
    features = hidden.shape[1]
    columns = value_weight.shape[1]
    ny = inner_size(sp)
    nz = sp // ny
    values = jnp.dot(hidden, value_weight, preferred_element_type=F32).astype(BF16)
    v = values.reshape(length, groups, per, head_width)
    cot = cotangent.reshape(length, groups, per, head_width)
    log_decay = -decay_rate[None, :] * jax.nn.softplus(decay_pre)
    tri = jnp.tril(jnp.ones((length, length), F32))
    cum = jnp.dot(tri, log_decay, precision=lax.Precision.HIGHEST)
    tot = cum[-1]
    to_end = jnp.exp(tot[None] - cum).reshape(length, groups, per, 1)
    ecum = jnp.exp(cum).reshape(length, groups, per, 1)
    local_state = two_pass("sgip,sgn->gipn", to_end * v.astype(F32), key_vecs)
    local_pull = two_pass("sgip,sgn->gipn", ecum * cot.astype(F32), queries)
    both = jnp.stack([local_state, local_pull], axis=2).reshape(heads, 2, head_width, state)
    dec = jnp.broadcast_to(jnp.exp(tot)[:, None, None], (heads, 1, state))
    span = features // nz
    scanned, hcol = pl.pallas_call(
        functools.partial(scan_kernel, ny, nz),
        out_shape=(
            jax.ShapeDtypeStruct(both.shape, F32),
            jax.ShapeDtypeStruct((nz * length, span), BF16),
        ),
        in_specs=[VM] * 3,
        out_specs=(VM, VM),
        scratch_shapes=[
            pltpu.VMEM((ny,) + both.shape, F32),
            pltpu.VMEM((ny,) + dec.shape, F32),
            pltpu.VMEM((2, heads, head_width, state), F32),
            pltpu.VMEM((2, heads, head_width, state), F32),
            pltpu.VMEM((length, features), F32),
            pltpu.VMEM((nz, length, span), F32),
            pltpu.SemaphoreType.DMA((ny, heads)),
            pltpu.SemaphoreType.DMA((ny, heads)),
            pltpu.SemaphoreType.DMA((ny,)),
            pltpu.SemaphoreType.DMA((ny,)),
            pltpu.SemaphoreType.DMA((2, heads)),
            pltpu.SemaphoreType.DMA((2, heads)),
            pltpu.SemaphoreType.DMA((nz,)),
            pltpu.SemaphoreType.DMA((nz,)),
        ],
        compiler_params=pltpu.CompilerParams(collective_id=0, has_side_effects=True, vmem_limit_bytes=LIMIT),
        name="scan_states",
    )(both, dec, hidden)
    state_in = scanned[:, 0].reshape(groups, per, head_width, state)
    state_grad = scanned[:, 1].reshape(groups, per, head_width, state)

    cum_h = cum.T
    causal = jnp.tril(jnp.ones((length, length), dtype=bool))[None]
    across = cum_h[:, :, None] - cum_h[:, None, :]
    damping = jnp.where(causal, jnp.exp(jnp.where(causal, across, 0.0)), 0.0).reshape(groups, per, length, length)
    scores = jnp.einsum("tgn,sgn->gts", queries, key_vecs, preferred_element_type=F32)
    pair = jnp.einsum("tgip,sgip->gits", cot, v, preferred_element_type=F32)
    dscore = pair * damping
    flux = dscore * scores[:, None]
    net = (jnp.sum(flux, axis=3) - jnp.sum(flux, axis=2)).reshape(heads, length).T
    dsum = jnp.sum(dscore, axis=1)
    mixed = (scores[:, None] * damping).astype(BF16)
    gq_heads = ecum * two_pass("gipn,tgip->tgin", state_in, cot)
    gk_heads = to_end * two_pass("gipn,tgip->tgin", state_grad, v)
    gv = jnp.einsum("gits,tgip->sgip", mixed, cot, preferred_element_type=F32) + to_end * two_pass(
        "gipn,sgn->sgip", state_grad, key_vecs
    )
    gq = two_pass("gts,sgn->tgn", dsum, key_vecs) + jnp.sum(gq_heads, axis=2)
    gk = two_pass("gts,tgn->sgn", dsum, queries) + jnp.sum(gk_heads, axis=2)
    qgq = jnp.sum(gq_heads * queries.astype(F32)[:, :, None], axis=3).reshape(length, heads)
    kgk = jnp.sum(gk_heads * key_vecs.astype(F32)[:, :, None], axis=3).reshape(length, heads)
    through = jnp.exp(tot) * jnp.sum(state_in * state_grad, axis=(2, 3)).reshape(heads)
    suffix = jnp.dot(tri.T, net + qgq, precision=lax.Precision.HIGHEST)
    prefix = jnp.dot(tri - jnp.eye(length, dtype=F32), kgk, precision=lax.Precision.HIGHEST)
    grad_decay = (suffix + prefix + through[None]) * -decay_rate[None] * jax.nn.sigmoid(decay_pre)

    grad_flat = gv.reshape(length, columns).astype(BF16)
    ghp = lax.dot_general(grad_flat, value_weight, (((1,), (1,)), ((), ())), preferred_element_type=F32)
    rows = features // sp
    width = min(columns, 128)
    chunks = columns // width
    grad_weight, grad_hidden = pl.pallas_call(
        functools.partial(grads_kernel, ny, nz, tp, width),
        out_shape=(
            jax.ShapeDtypeStruct((rows, columns), F32),
            jax.ShapeDtypeStruct((length // tp, features), BF16),
        ),
        in_specs=[VM] * 3,
        out_specs=(VM, VM),
        scratch_shapes=[
            pltpu.VMEM((nz, chunks, length, width), F32),
            pltpu.VMEM((ny, chunks, rows, width), F32),
            pltpu.VMEM((ny, chunks, rows, width), F32),
            pltpu.VMEM((tp, length // tp, features), F32),
            pltpu.SemaphoreType.DMA((nz, chunks)),
            pltpu.SemaphoreType.DMA((nz, chunks)),
            pltpu.SemaphoreType.DMA((nz, chunks)),
            pltpu.SemaphoreType.DMA((ny, chunks)),
            pltpu.SemaphoreType.DMA((ny, chunks)),
            pltpu.SemaphoreType.DMA((tp,)),
            pltpu.SemaphoreType.DMA((tp,)),
        ],
        compiler_params=pltpu.CompilerParams(collective_id=1, has_side_effects=True, vmem_limit_bytes=LIMIT),
        name="weight_grads",
    )(grad_flat.astype(F32), hcol.T, ghp)
    return (gq_cast(gk), gq_cast(gq), grad_decay, grad_hidden, grad_weight)


def gq_cast(x):
    return x.astype(BF16)


def solution(mesh):
    return jax.shard_map(
        functools.partial(per_device, mesh.shape["sp"], mesh.shape["tp"]),
        mesh=mesh,
        in_specs=(
            P("sp", None),
            P(None, "tp"),
            P("sp", "tp", None),
            P("sp", "tp", None),
            P("sp", "tp"),
            P("tp"),
            P("sp", "tp", None),
        ),
        out_specs=(
            P("sp", "tp", None),
            P("sp", "tp", None),
            P("sp", "tp"),
            P(("sp", "tp"), None),
            P("sp", "tp"),
        ),
        check_vma=False,
    )
```

time: 361 us -> 144 us (0.40)
  waiting for transfers between devices: 251 us -> 0 us
  Pallas kernels: 0 us -> 124 us
  matrix products: 53 us -> 13.1 us
  blocking collectives: 22.4 us -> 0 us
  between operations: 14 us -> 0.95 us
  local copies, waits for them, and re-layouts: 12.9 us -> 5.29 us
  other arithmetic: 7.52 us -> 0.63 us
    reduce_scatter x2 -> x0, waiting for transfers between devices: 133 us -> none  [summed_rows(): own = lax.psum_scatter(everything, axis, scatter_dimension=0, tiled=True)]
    pallas_call x0 -> x2, Pallas kernels: none -> 124 us  [the longest x1 73.7 us: per_device(): pl.pallas_call(functools.partial(scan_kernel, ny, nz), out_shape=(jax.Sha...]
    all_gather x2 -> x0, waiting for transfers between devices: 117 us -> none  [over_all(): lax.all_gather(part, axis, axis=dim, tiled=True)]
    dot_general x16 -> x22, matrix products: 53 us -> 13.1 us  [the longest x1 3.71 us: per_device(): lax.dot_general(grad_flat, value_weight, (((1,), (1,)), ((), ())), prefer...]
    all_gather x1 -> x0, blocking collectives: 22.4 us -> none  [per_device(): totals = lax.all_gather(decay_total[None, :], 'sp', axis=0, tiled=True)]
    unnamed x38 -> x16, local copies, waits for them, and re-layouts: 7.82 us -> 3.06 us
  transfers between devices with their start and end apart: 4 -> 0, of which waited for: 4 -> 0; matrix products, arithmetic and copies ran while one was open for 13% -> 0% of each run, Pallas kernels for 0% -> 0%
where the time goes in v1:
time: 144 us
  Pallas kernels  124 us (86%)
  matrix products  13.1 us (9%)
  local copies, waits for them, and re-layouts  5.29 us (4%)
    pallas_call x1, Pallas kernels, per_device(): pl.pallas_call(functools.partial(scan_kernel, ny, nz), out_shape=(jax.Sha...  73.7 us
    pallas_call x1, Pallas kernels, per_device(): pl.pallas_call(functools.partial(grads_kernel, ny, nz, tp, width), out_sh...  50.5 us
    dot_general x1, matrix products, per_device(): lax.dot_general(grad_flat, value_weight, (((1,), (1,)), ((), ())), prefer...  3.71 us
    dot_general x1, matrix products, per_device(): jnp.dot(hidden, value_weight, preferred_element_type=F32).astype(BF16)  3.07 us
    unnamed x16, local copies, waits for them, and re-layouts  3.06 us

profile of v1, /device:TPU:0, one launch (start us, length us, event | category | flops | bytes accessed | tf_op | source)
XLA Modules:
  0.0 144.2 jit_solution(8678232495104255380)
XLA Ops:
  0.6 0.0 copy-start.2
  0.7 1.0 copy.80
  1.7 3.1 %convolution_convert_fusion = bf16[128,1024]{1,0:T(8,128)(2,1)S(1)} fusion(bf16[128,2048]{1,0:T(8,128)(2,1)} %hid_ref.1, bf16[2048,1024]{1,0:T(8,128)(2,1)} %param.8), kind=kOutput, calls=%fused_computation.16 | convolution fusion | flops 537001984 | bytes 4980736 | tf_op jit(solution)/shard_map/dot_general | solution.py:355
  4.8 0.0 copy-start
  4.8 0.2 copy.63
  5.0 0.0 copy-done.5
  5.0 0.2 fusion.40
  5.2 0.2 slice_reduce_fusion
  5.4 0.1 exponential_bitcast_fusion.1
  5.5 0.0 copy-done.1
  5.5 0.0 copy-done.3
  5.5 0.2 fusion.31
  5.7 0.2 convolution_add_fusion.3
  6.0 0.2 fusion.30
  6.2 0.2 convolution_add_fusion.4
  6.4 0.1 pad_maximum_fusion.both_ref
  6.5 0.1 broadcast_in_dim.48.dec_ref
  6.6 0.0 copy-done
  6.6 73.7 %scan_states.1 = (f32[16,2,64,128]{3,2,1,0:T(8,128)S(1)}, bf16[512,512]{1,0:T(8,128)(2,1)S(1)}) custom-call(f32[16,2,64,128]{3,2,1,0:T(8,128)S(1)} %pad_maximum_fusion.both_ref, f32[16,1,128]{2,1,0:T(1,128)S(1)} %broadcast_in_dim.48.dec_ref, bf16[128,2048]{1,0:T(8,128)(2,1)S(1)} %copy-done), custom_call_target="tpu_custom_call" | custom-call | tf_op jit(solution)/shard_map/scan_states/pallas_call | solution.py:369
  80.3 0.2 multiply_reduce_fusion.4
  80.5 0.3 fusion.43
  80.9 0.4 multiply_reduce_fusion
  81.3 0.1 copy.70
  81.4 0.2 fusion.49
  81.6 0.9 multiply_reduce_fusion.2
  82.4 0.1 fusion.56
  82.6 0.2 fusion.14
  82.7 0.7 copy.87
  83.4 0.1 copy.79
  83.6 0.4 fusion.32
  83.9 0.4 multiply_reduce_fusion.1
  84.3 0.1 copy.75
  84.4 0.2 fusion.52
  84.6 0.2 fusion.13
  84.9 0.7 copy.88
  85.6 0.2 fusion.38
  85.8 0.1 copy.81
  85.9 0.2 multiply_reduce_fusion.5
  86.1 0.8 fusion.17
  86.9 0.5 convolution_bitcast_fusion.1
  87.4 0.2 fusion.42
  87.7 0.2 fusion.8
  87.9 0.1 copy.85
  88.1 0.2 copy.86
  88.3 3.7 %fusion.90.ghp_ref = f32[128,2048]{1,0:T(8,128)S(1)} fusion(bf16[128,1024]{0,1:T(8,128)(2,1)S(1)} %bitcast.131, bf16[2048,1024]{1,0:T(8,128)(2,1)} %param.8), kind=kOutput, calls=%fused_computation.122 | convolution fusion | flops 536870912 | bytes 5505024 | tf_op jit(solution)/shard_map/dot_general | solution.py:425
  92.0 50.5 %weight_grads.1 = (f32[256,1024]{1,0:T(8,128)S(1)}, bf16[32,2048]{1,0:T(8,128)(2,1)S(1)}) custom-call(f32[128,1024]{1,0:T(8,128)S(1)} %convert_element_type.91.gv_ref, bf16[512,512]{1,0:T(8,128)(2,1)S(1)} %bitcast.106, f32[128,2048]{1,0:T(8,128)S(1)} %fusion.90.ghp_ref), custom_call_target="tpu_custom_call" | custom-call | tf_op jit(solution)/shard_map/weight_grads/pallas_call | solution.py:429
  142.6 0.7 copy.137
  143.2 1.0 copy.138
  (10 shorter events, 0.1 us)
Async XLA Ops:
  0.6 5.3 %copy-start.2 = (bf16[128,2,128]{2,1,0:T(2,128)(2,1)S(1)}, bf16[128,2,128]{2,1,0:T(2,128)(2,1)}, u32[]{:S(2)}) copy-start(bf16[128,2,128]{2,1,0:T(2,128)(2,1)} %param.9) | copy-start | bytes 196612
  0.6 4.8 %copy-start.1 = (bf16[128,16,64]{0,2,1:T(8,128)(2,1)S(1)}, bf16[128,16,64]{0,2,1:T(8,128)(2,1)}, u32[]{:S(2)}) copy-start(bf16[128,16,64]{0,2,1:T(8,128)(2,1)} %param.13) | copy-start | bytes 786436
  0.7 4.3 %copy-start.4 = (f32[128,16]{0,1:T(8,128)S(1)}, f32[128,16]{0,1:T(8,128)}, u32[]{:S(2)}) copy-start(f32[128,16]{0,1:T(8,128)} %param.11) | copy-start | bytes 24580
  0.7 4.3 %copy-start.5 = (f32[16]{0:T(128)S(1)}, f32[16]{0:T(128)}, u32[]{:S(2)}) copy-start(f32[16]{0:T(128)} %param.12) | copy-start | bytes 196
  0.7 4.8 %copy-start.3 = (bf16[128,2,128]{2,1,0:T(2,128)(2,1)S(1)}, bf16[128,2,128]{2,1,0:T(2,128)(2,1)}, u32[]{:S(2)}) copy-start(bf16[128,2,128]{2,1,0:T(2,128)(2,1)} %param.10) | copy-start | bytes 196612
  4.8 1.8 %copy-start = (bf16[128,2048]{1,0:T(8,128)(2,1)S(1)}, bf16[128,2048]{1,0:T(8,128)(2,1)}, u32[]{:S(2)}) copy-start(bf16[128,2048]{1,0:T(8,128)(2,1)} %hid_ref.1) | copy-start | bytes 1572868

commit v2 on v1

--- a/solution.py
+++ b/solution.py
@@ -27,9 +27,9 @@
     )
 
 
-def scan_kernel(ny, nz, both_ref, dec_ref, hid_ref, out_ref, hcol_ref,
+def scan_kernel(ny, nz, ntp, skew, pieces, both_ref, dec_ref, hid_ref, out_ref, hcol_ref,
                 ybuf, ydec, pin, pout, hid_f, hland,
-                ysend, yrecv, dsend, drecv, psend, precv, hsend, hrecv):
+                ysend, yrecv, dsend, drecv, psend, precv, hsend, hrecv, fsend, frecv):
     me = lax.axis_index("sp")
     z, y = me // ny, me % ny
     heads = both_ref.shape[0]
@@ -40,7 +40,15 @@
         pl.semaphore_signal(barrier, inc=1, device_id={"sp": z * ny + (y + dy) % ny}, device_id_type=MESH)
     for dz in range(1, nz):
         pl.semaphore_signal(barrier, inc=1, device_id={"sp": ((z + dz) % nz) * ny + y}, device_id_type=MESH)
-    pl.semaphore_wait(barrier, ny - 1 + nz - 1)
+    mine = lax.axis_index("tp")
+    halves = 2 if ntp % 2 == 0 else 1
+    half = mine % halves
+    other = mine + 1 - 2 * half
+    if halves == 2:
+        pl.semaphore_signal(barrier, inc=1, device_id={"tp": other}, device_id_type=MESH)
+    pl.semaphore_wait(barrier, ny - 1 + nz - 1 + halves - 1)
+    half_rows = hland.shape[1] // halves
+    piece_rows = half_rows // pieces
 
     def ycopy(h, dy):
         there = (y + dy) % ny
@@ -67,23 +75,32 @@
 
     lax.fori_loop(0, heads, launch, 0)
 
-    def hcopy(dz):
+    def piece(p):
+        return pl.ds(pl.multiple_of(half * half_rows + p * piece_rows, 8), piece_rows)
+
+    def columns_of(plane):
+        return pl.ds(pl.multiple_of(plane * span, 128), span)
+
+    def hcopy(dz, p):
         there = (z + dz) % nz
         return remote(
-            hid_f.at[:, pl.ds(pl.multiple_of(there * span, 128), span)], hland.at[z],
-            hsend.at[there], hrecv.at[z], "sp", there * ny + y,
-        )
-
-    def harrive(dz):
+            hid_f.at[piece(p), columns_of(there)], hland.at[z, piece(p)],
+            hsend.at[there, p], hrecv.at[z, p], "sp", there * ny + y,
+        )
+
+    def harrive(dz, p):
         there = (z + dz) % nz
         return remote(
-            hid_f.at[:, pl.ds(pl.multiple_of(there * span, 128), span)], hland.at[there],
-            hsend.at[there], hrecv.at[there], "sp", there * ny + y,
-        )
+            hid_f.at[piece(p), columns_of(there)], hland.at[there, piece(p)],
+            hsend.at[there, p], hrecv.at[there, p], "sp", there * ny + y,
+        )
+
+    def share(dz, part):
+        there = (z + dz) % nz
+        block = hland.at[there, pl.ds(pl.multiple_of(part * half_rows, 8), half_rows)]
+        return remote(block, block, fsend.at[there], frecv.at[there], "tp", other)
 
     hid_f[...] = hid_ref[...].astype(F32)
-    for dz in range(1, nz):
-        hcopy(dz).start()
     ybuf[y] = both_ref[...]
     ydec[y] = dec_ref[...]
     for dy in range(1, ny):
@@ -110,8 +127,8 @@
                 yarrive(h, (y + dy) % ny).wait_recv()
 
     def step(t, carry):
-        a = t - z
-        b = t - (nz - 1 - z)
+        a = t - skew * z
+        b = t - skew * (nz - 1 - z)
 
         @pl.when((a >= 0) & (a < heads))
         def _():
@@ -155,19 +172,33 @@
             def _():
                 down(b).start()
 
-        return carry
-
-    lax.fori_loop(0, heads + nz - 1, step, 0)
+        @pl.when(t < pieces * (nz - 1))
+        def _():
+            hcopy(1 + t // pieces, t % pieces).start()
+
+        return carry
+
+    lax.fori_loop(0, max(heads + skew * (nz - 1), pieces * (nz - 1)), step, 0)
+
+    for dz in range(1, nz):
+        for p in range(pieces):
+            harrive(dz, p).wait_recv()
+        if halves == 2:
+            share(dz, half).start()
 
     hcol_ref[pl.ds(pl.multiple_of(z * hland.shape[1], 128), hland.shape[1]), :] = (
         hid_f[:, pl.ds(pl.multiple_of(z * span, 128), span)].astype(BF16)
     )
     for dz in range(1, nz):
         there = (z + dz) % nz
-        harrive(dz).wait_recv()
+        if halves == 2:
+            share(dz, 1 - half).wait_recv()
         hcol_ref[pl.ds(pl.multiple_of(there * hland.shape[1], 128), hland.shape[1]), :] = hland[there].astype(BF16)
     for dz in range(1, nz):
-        hcopy(dz).wait_send()
+        for p in range(pieces):
+            hcopy(dz, p).wait_send()
+        if halves == 2:
+            share(dz, half).wait_send()
     for dy in range(1, ny):
         dcopy(dy).wait_send()
 
@@ -366,8 +397,9 @@
     both = jnp.stack([local_state, local_pull], axis=2).reshape(heads, 2, head_width, state)
     dec = jnp.broadcast_to(jnp.exp(tot)[:, None, None], (heads, 1, state))
     span = features // nz
+    pieces = 4
     scanned, hcol = pl.pallas_call(
-        functools.partial(scan_kernel, ny, nz),
+        functools.partial(scan_kernel, ny, nz, tp, 3, pieces),
         out_shape=(
             jax.ShapeDtypeStruct(both.shape, F32),
             jax.ShapeDtypeStruct((nz * length, span), BF16),
@@ -387,6 +419,8 @@
             pltpu.SemaphoreType.DMA((ny,)),
             pltpu.SemaphoreType.DMA((2, heads)),
             pltpu.SemaphoreType.DMA((2, heads)),
+            pltpu.SemaphoreType.DMA((nz, pieces)),
+            pltpu.SemaphoreType.DMA((nz, pieces)),
             pltpu.SemaphoreType.DMA((nz,)),
             pltpu.SemaphoreType.DMA((nz,)),
         ],
@@ -406,10 +440,10 @@
     flux = dscore * scores[:, None]
     net = (jnp.sum(flux, axis=3) - jnp.sum(flux, axis=2)).reshape(heads, length).T
     dsum = jnp.sum(dscore, axis=1)
-    mixed = (scores[:, None] * damping).astype(BF16)
+    mixed = scores[:, None] * damping
     gq_heads = ecum * two_pass("gipn,tgip->tgin", state_in, cot)
     gk_heads = to_end * two_pass("gipn,tgip->tgin", state_grad, v)
-    gv = jnp.einsum("gits,tgip->sgip", mixed, cot, preferred_element_type=F32) + to_end * two_pass(
+    gv = two_pass("gits,tgip->sgip", mixed, cot) + to_end * two_pass(
         "gipn,sgn->sgip", state_grad, key_vecs
     )
     gq = two_pass("gts,sgn->tgn", dsum, key_vecs) + jnp.sum(gq_heads, axis=2)

time: 144 us -> 115 us (0.80)
  Pallas kernels: 124 us -> 94.5 us
    pallas_call x1, Pallas kernels: 73.7 us -> 44.5 us  [per_device(): pl.pallas_call(functools.partial(scan_kernel, ny, nz, tp, 3, pieces), out...]
where the time goes in v2:
time: 115 us
  Pallas kernels  94.5 us (82%)
  matrix products  13.7 us (12%)
  local copies, waits for them, and re-layouts  5.29 us (5%)
    pallas_call x1, Pallas kernels, per_device(): pl.pallas_call(functools.partial(grads_kernel, ny, nz, tp, width), out_sh...  50 us
    pallas_call x1, Pallas kernels, per_device(): pl.pallas_call(functools.partial(scan_kernel, ny, nz, tp, 3, pieces), out...  44.5 us
    dot_general x1, matrix products, per_device(): lax.dot_general(grad_flat, value_weight, (((1,), (1,)), ((), ())), prefer...  3.71 us
    dot_general x1, matrix products, per_device(): jnp.dot(hidden, value_weight, preferred_element_type=F32).astype(BF16)  3.07 us
    unnamed x16, local copies, waits for them, and re-layouts  3.06 us
    dot_general x8, matrix products, two_pass(): jnp.einsum(spec, lo, y, preferred_element_type=F32)  2.49 us

profile of v2, /device:TPU:0, one launch (start us, length us, event | category | flops | bytes accessed | tf_op | source)
XLA Modules:
  0.0 115.0 jit_solution(15734864825274293283)
XLA Ops:
  0.6 0.0 copy-start.2
  0.6 0.0 copy-start.1
  0.7 1.0 copy.82
  1.7 3.1 %convolution_convert_fusion = bf16[128,1024]{1,0:T(8,128)(2,1)S(1)} fusion(bf16[128,2048]{1,0:T(8,128)(2,1)} %hid_ref.1, bf16[2048,1024]{1,0:T(8,128)(2,1)} %param.8), kind=kOutput, calls=%fused_computation.19 | convolution fusion | flops 537001984 | bytes 4980736 | tf_op jit(solution)/shard_map/dot_general | solution.py:386
  4.8 0.0 copy-start
  4.8 0.2 copy.65
  5.0 0.2 fusion.50
  5.2 0.2 slice_reduce_fusion
  5.4 0.1 exponential_bitcast_fusion.1
  5.5 0.0 copy-done.3
  5.5 0.2 fusion.41
  5.7 0.2 convolution_add_fusion.3
  6.0 0.2 fusion.40
  6.2 0.2 convolution_add_fusion.4
  6.4 0.1 pad_maximum_fusion.both_ref
  6.5 0.1 broadcast_in_dim.48.dec_ref
  6.6 0.0 copy-done
  6.6 44.5 %scan_states.1 = (f32[16,2,64,128]{3,2,1,0:T(8,128)S(1)}, bf16[512,512]{1,0:T(8,128)(2,1)S(1)}) custom-call(f32[16,2,64,128]{3,2,1,0:T(8,128)S(1)} %pad_maximum_fusion.both_ref, f32[16,1,128]{2,1,0:T(1,128)S(1)} %broadcast_in_dim.48.dec_ref, bf16[128,2048]{1,0:T(8,128)(2,1)S(1)} %copy-done), custom_call_target="tpu_custom_call" | custom-call | tf_op jit(solution)/shard_map/scan_states/pallas_call | solution.py:401
  51.1 0.2 multiply_reduce_fusion.4
  51.3 0.4 fusion.53
  51.6 0.4 multiply_reduce_fusion
  52.1 0.1 copy.72
  52.2 0.2 fusion.59
  52.3 0.9 multiply_reduce_fusion.2
  53.2 0.1 fusion.66
  53.4 0.2 fusion.15
  53.5 0.7 copy.90
  54.2 0.1 copy.81
  54.3 0.4 fusion.42
  54.7 0.4 multiply_reduce_fusion.1
  55.1 0.1 copy.77
  55.2 0.2 fusion.62
  55.4 0.2 fusion.14
  55.7 0.7 copy.91
  56.4 0.2 fusion.48
  56.5 0.1 copy.83
  56.7 0.2 multiply_reduce_fusion.5
  56.9 0.8 fusion.18
  57.7 0.5 fusion.22
  58.2 0.6 fusion.8
  58.8 0.2 fusion.52
  59.0 0.2 fusion.9
  59.3 0.1 copy.88
  59.5 0.2 copy.89
  59.7 3.7 %fusion.101.ghp_ref = f32[128,2048]{1,0:T(8,128)S(1)} fusion(bf16[128,1024]{0,1:T(8,128)(2,1)S(1)} %bitcast.133, bf16[2048,1024]{1,0:T(8,128)(2,1)} %param.8), kind=kOutput, calls=%fused_computation.133 | convolution fusion | flops 536870912 | bytes 5505024 | tf_op jit(solution)/shard_map/dot_general | solution.py:459
  63.4 50.0 %weight_grads.1 = (f32[256,1024]{1,0:T(8,128)S(1)}, bf16[32,2048]{1,0:T(8,128)(2,1)S(1)}) custom-call(f32[128,1024]{1,0:T(8,128)S(1)} %convert_element_type.95.gv_ref, bf16[512,512]{1,0:T(8,128)(2,1)S(1)} %bitcast.107, f32[128,2048]{1,0:T(8,128)S(1)} %fusion.101.ghp_ref), custom_call_target="tpu_custom_call" | custom-call | tf_op jit(solution)/shard_map/weight_grads/pallas_call | solution.py:463
  113.4 0.7 copy.141
  114.1 1.0 copy.142
  (11 shorter events, 0.1 us)
Async XLA Ops:
  0.6 5.3 %copy-start.2 = (bf16[128,2,128]{2,1,0:T(2,128)(2,1)S(1)}, bf16[128,2,128]{2,1,0:T(2,128)(2,1)}, u32[]{:S(2)}) copy-start(bf16[128,2,128]{2,1,0:T(2,128)(2,1)} %param.9) | copy-start | bytes 196612
  0.6 4.8 %copy-start.1 = (bf16[128,16,64]{0,2,1:T(8,128)(2,1)S(1)}, bf16[128,16,64]{0,2,1:T(8,128)(2,1)}, u32[]{:S(2)}) copy-start(bf16[128,16,64]{0,2,1:T(8,128)(2,1)} %param.13) | copy-start | bytes 786436
  0.7 4.3 %copy-start.4 = (f32[128,16]{0,1:T(8,128)S(1)}, f32[128,16]{0,1:T(8,128)}, u32[]{:S(2)}) copy-start(f32[128,16]{0,1:T(8,128)} %param.11) | copy-start | bytes 24580
  0.7 4.3 %copy-start.5 = (f32[16]{0:T(128)S(1)}, f32[16]{0:T(128)}, u32[]{:S(2)}) copy-start(f32[16]{0:T(128)} %param.12) | copy-start | bytes 196
  0.7 4.8 %copy-start.3 = (bf16[128,2,128]{2,1,0:T(2,128)(2,1)S(1)}, bf16[128,2,128]{2,1,0:T(2,128)(2,1)}, u32[]{:S(2)}) copy-start(bf16[128,2,128]{2,1,0:T(2,128)(2,1)} %param.10) | copy-start | bytes 196612
  4.8 1.8 %copy-start = (bf16[128,2048]{1,0:T(8,128)(2,1)S(1)}, bf16[128,2048]{1,0:T(8,128)(2,1)}, u32[]{:S(2)}) copy-start(bf16[128,2048]{1,0:T(8,128)(2,1)} %hid_ref.1) | copy-start | bytes 1572868

commit v3 on v2

--- a/solution.py
+++ b/solution.py
@@ -261,7 +261,8 @@
 
         return carry
 
-    lax.fori_loop(0, chunks, launch, 0)
+    ahead = min(2, chunks)
+    lax.fori_loop(0, ahead, launch, 0)
 
     def hcopy(dt):
         there = (mine + dt) % ntp
@@ -309,6 +310,10 @@
                 @pl.when(z > 0)
                 def _():
                     down(jnp.minimum(high, nz - 1), c).start()
+
+        @pl.when(c + ahead < chunks)
+        def _():
+            launch(c + ahead, 0)
 
         block = gath[:, c].reshape(nz * length, width).astype(BF16)
         for dy in range(1, ny):
@@ -399,7 +404,7 @@
     span = features // nz
     pieces = 4
     scanned, hcol = pl.pallas_call(
-        functools.partial(scan_kernel, ny, nz, tp, 3, pieces),
+        functools.partial(scan_kernel, ny, nz, tp, 2, pieces),
         out_shape=(
             jax.ShapeDtypeStruct(both.shape, F32),
             jax.ShapeDtypeStruct((nz * length, span), BF16),

time: 115 us -> 121 us (1.052)
  Pallas kernels: 94.5 us -> 99.7 us
    pallas_call x1, Pallas kernels: 44.5 us -> 47.1 us  [per_device(): pl.pallas_call(functools.partial(scan_kernel, ny, nz, tp, 2, pieces), out...]
    pallas_call x1, Pallas kernels: 50 us -> 52.6 us  [per_device(): pl.pallas_call(functools.partial(grads_kernel, ny, nz, tp, width), out_sh...]
where the time goes in v3:
time: 121 us; the launch traced here: 120 us
  Pallas kernels  99.7 us (82%)
  matrix products  13.7 us (11%)
  local copies, waits for them, and re-layouts  5.29 us (4%)
    pallas_call x1, Pallas kernels, per_device(): pl.pallas_call(functools.partial(grads_kernel, ny, nz, tp, width), out_sh...  52.6 us
    pallas_call x1, Pallas kernels, per_device(): pl.pallas_call(functools.partial(scan_kernel, ny, nz, tp, 2, pieces), out...  47.1 us
    dot_general x1, matrix products, per_device(): lax.dot_general(grad_flat, value_weight, (((1,), (1,)), ((), ())), prefer...  3.71 us
    dot_general x1, matrix products, per_device(): jnp.dot(hidden, value_weight, preferred_element_type=F32).astype(BF16)  3.07 us
    unnamed x16, local copies, waits for them, and re-layouts  3.06 us
    dot_general x8, matrix products, two_pass(): jnp.einsum(spec, lo, y, preferred_element_type=F32)  2.49 us

profile of v3, /device:TPU:0, one launch (start us, length us, event | category | flops | bytes accessed | tf_op | source)
XLA Modules:
  0.0 120.3 jit_solution(2359227422099422582)
XLA Ops:
  0.6 0.0 copy-start.2
  0.7 1.0 copy.82
  1.7 3.1 %convolution_convert_fusion = bf16[128,1024]{1,0:T(8,128)(2,1)S(1)} fusion(bf16[128,2048]{1,0:T(8,128)(2,1)} %hid_ref.1, bf16[2048,1024]{1,0:T(8,128)(2,1)} %param.8), kind=kOutput, calls=%fused_computation.19 | convolution fusion | flops 537001984 | bytes 4980736 | tf_op jit(solution)/shard_map/dot_general | solution.py:391
  4.8 0.0 copy-start
  4.8 0.2 copy.65
  5.0 0.0 copy-done.4
  5.0 0.2 fusion.50
  5.2 0.2 slice_reduce_fusion
  5.4 0.1 exponential_bitcast_fusion.1
  5.5 0.0 copy-done.3
  5.5 0.2 fusion.41
  5.7 0.2 convolution_add_fusion.3
  6.0 0.2 fusion.40
  6.2 0.2 convolution_add_fusion.4
  6.4 0.1 pad_maximum_fusion.both_ref
  6.5 0.1 broadcast_in_dim.48.dec_ref
  6.6 0.0 copy-done
  6.6 47.1 %scan_states.1 = (f32[16,2,64,128]{3,2,1,0:T(8,128)S(1)}, bf16[512,512]{1,0:T(8,128)(2,1)S(1)}) custom-call(f32[16,2,64,128]{3,2,1,0:T(8,128)S(1)} %pad_maximum_fusion.both_ref, f32[16,1,128]{2,1,0:T(1,128)S(1)} %broadcast_in_dim.48.dec_ref, bf16[128,2048]{1,0:T(8,128)(2,1)S(1)} %copy-done), custom_call_target="tpu_custom_call" | custom-call | tf_op jit(solution)/shard_map/scan_states/pallas_call | solution.py:406
  53.7 0.2 multiply_reduce_fusion.4
  54.0 0.4 fusion.53
  54.3 0.4 multiply_reduce_fusion
  54.7 0.1 copy.72
  54.8 0.2 fusion.59
  55.0 0.9 multiply_reduce_fusion.2
  55.9 0.1 fusion.66
  56.0 0.2 fusion.15
  56.2 0.7 copy.90
  56.9 0.1 copy.81
  57.0 0.4 fusion.42
  57.4 0.4 multiply_reduce_fusion.1
  57.8 0.1 copy.77
  57.9 0.2 fusion.62
  58.1 0.2 fusion.14
  58.3 0.7 copy.91
  59.0 0.2 fusion.48
  59.2 0.1 copy.83
  59.3 0.2 multiply_reduce_fusion.5
  59.5 0.8 fusion.18
  60.3 0.5 fusion.22
  60.9 0.6 fusion.8
  61.5 0.2 fusion.52
  61.7 0.2 fusion.9
  61.9 0.1 copy.88
  62.1 0.2 copy.89
  62.4 3.7 %fusion.101.ghp_ref = f32[128,2048]{1,0:T(8,128)S(1)} fusion(bf16[128,1024]{0,1:T(8,128)(2,1)S(1)} %bitcast.133, bf16[2048,1024]{1,0:T(8,128)(2,1)} %param.8), kind=kOutput, calls=%fused_computation.133 | convolution fusion | flops 536870912 | bytes 5505024 | tf_op jit(solution)/shard_map/dot_general | solution.py:464
  66.1 52.6 %weight_grads.1 = (f32[256,1024]{1,0:T(8,128)S(1)}, bf16[32,2048]{1,0:T(8,128)(2,1)S(1)}) custom-call(f32[128,1024]{1,0:T(8,128)S(1)} %convert_element_type.95.gv_ref, bf16[512,512]{1,0:T(8,128)(2,1)S(1)} %bitcast.107, f32[128,2048]{1,0:T(8,128)S(1)} %fusion.101.ghp_ref), custom_call_target="tpu_custom_call" | custom-call | tf_op jit(solution)/shard_map/weight_grads/pallas_call | solution.py:468
  118.7 0.7 copy.141
  119.4 1.0 copy.142
  (11 shorter events, 0.1 us)
Async XLA Ops:
  0.6 5.3 %copy-start.2 = (bf16[128,2,128]{2,1,0:T(2,128)(2,1)S(1)}, bf16[128,2,128]{2,1,0:T(2,128)(2,1)}, u32[]{:S(2)}) copy-start(bf16[128,2,128]{2,1,0:T(2,128)(2,1)} %param.9) | copy-start | bytes 196612
  0.6 4.8 %copy-start.1 = (bf16[128,16,64]{0,2,1:T(8,128)(2,1)S(1)}, bf16[128,16,64]{0,2,1:T(8,128)(2,1)}, u32[]{:S(2)}) copy-start(bf16[128,16,64]{0,2,1:T(8,128)(2,1)} %param.13) | copy-start | bytes 786436
  0.7 4.3 %copy-start.4 = (f32[128,16]{0,1:T(8,128)S(1)}, f32[128,16]{0,1:T(8,128)}, u32[]{:S(2)}) copy-start(f32[128,16]{0,1:T(8,128)} %param.11) | copy-start | bytes 24580
  0.7 4.3 %copy-start.5 = (f32[16]{0:T(128)S(1)}, f32[16]{0:T(128)}, u32[]{:S(2)}) copy-start(f32[16]{0:T(128)} %param.12) | copy-start | bytes 196
  0.7 4.8 %copy-start.3 = (bf16[128,2,128]{2,1,0:T(2,128)(2,1)S(1)}, bf16[128,2,128]{2,1,0:T(2,128)(2,1)}, u32[]{:S(2)}) copy-start(bf16[128,2,128]{2,1,0:T(2,128)(2,1)} %param.10) | copy-start | bytes 196612
  4.8 1.8 %copy-start = (bf16[128,2048]{1,0:T(8,128)(2,1)S(1)}, bf16[128,2048]{1,0:T(8,128)(2,1)}, u32[]{:S(2)}) copy-start(bf16[128,2048]{1,0:T(8,128)(2,1)} %hid_ref.1) | copy-start | bytes 1572868

commit v4 on v3

--- a/solution.py
+++ b/solution.py
@@ -261,7 +261,7 @@
 
         return carry
 
-    ahead = min(2, chunks)
+    ahead = min(5, chunks)
     lax.fori_loop(0, ahead, launch, 0)
 
     def hcopy(dt):
@@ -404,7 +404,7 @@
     span = features // nz
     pieces = 4
     scanned, hcol = pl.pallas_call(
-        functools.partial(scan_kernel, ny, nz, tp, 2, pieces),
+        functools.partial(scan_kernel, ny, nz, tp, 4, pieces),
         out_shape=(
             jax.ShapeDtypeStruct(both.shape, F32),
             jax.ShapeDtypeStruct((nz * length, span), BF16),

time: 121 us -> 109 us (0.901)
  Pallas kernels: 99.7 us -> 88.3 us
    pallas_call x1, Pallas kernels: 47.1 us -> 40.6 us  [per_device(): pl.pallas_call(functools.partial(scan_kernel, ny, nz, tp, 4, pieces), out...]
    pallas_call x1, Pallas kernels: 52.6 us -> 47.7 us  [per_device(): pl.pallas_call(functools.partial(grads_kernel, ny, nz, tp, width), out_sh...]
where the time goes in v4:
time: 109 us
  Pallas kernels  88.3 us (81%)
  matrix products  13.7 us (13%)
  local copies, waits for them, and re-layouts  5.29 us (5%)
    pallas_call x1, Pallas kernels, per_device(): pl.pallas_call(functools.partial(grads_kernel, ny, nz, tp, width), out_sh...  47.7 us
    pallas_call x1, Pallas kernels, per_device(): pl.pallas_call(functools.partial(scan_kernel, ny, nz, tp, 4, pieces), out...  40.6 us
    dot_general x1, matrix products, per_device(): lax.dot_general(grad_flat, value_weight, (((1,), (1,)), ((), ())), prefer...  3.71 us
    dot_general x1, matrix products, per_device(): jnp.dot(hidden, value_weight, preferred_element_type=F32).astype(BF16)  3.07 us
    unnamed x16, local copies, waits for them, and re-layouts  3.06 us
    dot_general x8, matrix products, two_pass(): jnp.einsum(spec, lo, y, preferred_element_type=F32)  2.49 us
    dot_general x8, matrix products, two_pass(): jnp.einsum(spec, hi, y, preferred_element_type=F32)  2.24 us

profile of v4, /device:TPU:0, one launch (start us, length us, event | category | flops | bytes accessed | tf_op | source)
XLA Modules:
  0.0 108.9 jit_solution(13468242875251917785)
XLA Ops:
  0.7 1.0 copy.82
  1.7 3.1 %convolution_convert_fusion = bf16[128,1024]{1,0:T(8,128)(2,1)S(1)} fusion(bf16[128,2048]{1,0:T(8,128)(2,1)} %hid_ref.1, bf16[2048,1024]{1,0:T(8,128)(2,1)} %param.8), kind=kOutput, calls=%fused_computation.19 | convolution fusion | flops 537001984 | bytes 4980736 | tf_op jit(solution)/shard_map/dot_general | solution.py:391
  4.8 0.0 copy-start
  4.8 0.2 copy.65
  5.0 0.0 copy-done.5
  5.0 0.2 fusion.50
  5.2 0.2 slice_reduce_fusion
  5.4 0.1 exponential_bitcast_fusion.1
  5.5 0.0 copy-done.1
  5.5 0.0 copy-done.3
  5.5 0.2 fusion.41
  5.7 0.2 convolution_add_fusion.3
  6.0 0.2 fusion.40
  6.2 0.2 convolution_add_fusion.4
  6.4 0.1 pad_maximum_fusion.both_ref
  6.5 0.1 broadcast_in_dim.48.dec_ref
  6.6 0.0 copy-done
  6.6 40.6 %scan_states.1 = (f32[16,2,64,128]{3,2,1,0:T(8,128)S(1)}, bf16[512,512]{1,0:T(8,128)(2,1)S(1)}) custom-call(f32[16,2,64,128]{3,2,1,0:T(8,128)S(1)} %pad_maximum_fusion.both_ref, f32[16,1,128]{2,1,0:T(1,128)S(1)} %broadcast_in_dim.48.dec_ref, bf16[128,2048]{1,0:T(8,128)(2,1)S(1)} %copy-done), custom_call_target="tpu_custom_call" | custom-call | tf_op jit(solution)/shard_map/scan_states/pallas_call | solution.py:406
  47.2 0.2 multiply_reduce_fusion.4
  47.4 0.3 fusion.53
  47.8 0.4 multiply_reduce_fusion
  48.2 0.1 copy.72
  48.3 0.2 fusion.59
  48.5 0.9 multiply_reduce_fusion.2
  49.3 0.1 fusion.66
  49.5 0.2 fusion.15
  49.7 0.7 copy.90
  50.4 0.1 copy.81
  50.5 0.4 fusion.42
  50.8 0.4 multiply_reduce_fusion.1
  51.2 0.1 copy.77
  51.3 0.2 fusion.62
  51.6 0.2 fusion.14
  51.8 0.7 copy.91
  52.5 0.2 fusion.48
  52.7 0.1 copy.83
  52.8 0.2 multiply_reduce_fusion.5
  53.0 0.8 fusion.18
  53.8 0.5 fusion.22
  54.3 0.6 fusion.8
  54.9 0.2 fusion.52
  55.1 0.2 fusion.9
  55.4 0.1 copy.88
  55.6 0.2 copy.89
  55.8 3.7 %fusion.101.ghp_ref = f32[128,2048]{1,0:T(8,128)S(1)} fusion(bf16[128,1024]{0,1:T(8,128)(2,1)S(1)} %bitcast.133, bf16[2048,1024]{1,0:T(8,128)(2,1)} %param.8), kind=kOutput, calls=%fused_computation.133 | convolution fusion | flops 536870912 | bytes 5505024 | tf_op jit(solution)/shard_map/dot_general | solution.py:464
  59.5 47.7 %weight_grads.1 = (f32[256,1024]{1,0:T(8,128)S(1)}, bf16[32,2048]{1,0:T(8,128)(2,1)S(1)}) custom-call(f32[128,1024]{1,0:T(8,128)S(1)} %convert_element_type.95.gv_ref, bf16[512,512]{1,0:T(8,128)(2,1)S(1)} %bitcast.107, f32[128,2048]{1,0:T(8,128)S(1)} %fusion.101.ghp_ref), custom_call_target="tpu_custom_call" | custom-call | tf_op jit(solution)/shard_map/weight_grads/pallas_call | solution.py:468
  107.3 0.7 copy.141
  107.9 1.0 copy.142
  (11 shorter events, 0.1 us)
Async XLA Ops:
  0.6 5.3 %copy-start.2 = (bf16[128,2,128]{2,1,0:T(2,128)(2,1)S(1)}, bf16[128,2,128]{2,1,0:T(2,128)(2,1)}, u32[]{:S(2)}) copy-start(bf16[128,2,128]{2,1,0:T(2,128)(2,1)} %param.9) | copy-start | bytes 196612
  0.6 4.8 %copy-start.1 = (bf16[128,16,64]{0,2,1:T(8,128)(2,1)S(1)}, bf16[128,16,64]{0,2,1:T(8,128)(2,1)}, u32[]{:S(2)}) copy-start(bf16[128,16,64]{0,2,1:T(8,128)(2,1)} %param.13) | copy-start | bytes 786436
  0.7 4.3 %copy-start.4 = (f32[128,16]{0,1:T(8,128)S(1)}, f32[128,16]{0,1:T(8,128)}, u32[]{:S(2)}) copy-start(f32[128,16]{0,1:T(8,128)} %param.11) | copy-start | bytes 24580
  0.7 4.3 %copy-start.5 = (f32[16]{0:T(128)S(1)}, f32[16]{0:T(128)}, u32[]{:S(2)}) copy-start(f32[16]{0:T(128)} %param.12) | copy-start | bytes 196
  0.7 4.8 %copy-start.3 = (bf16[128,2,128]{2,1,0:T(2,128)(2,1)S(1)}, bf16[128,2,128]{2,1,0:T(2,128)(2,1)}, u32[]{:S(2)}) copy-start(bf16[128,2,128]{2,1,0:T(2,128)(2,1)} %param.10) | copy-start | bytes 196612
  4.8 1.8 %copy-start = (bf16[128,2048]{1,0:T(8,128)(2,1)S(1)}, bf16[128,2048]{1,0:T(8,128)(2,1)}, u32[]{:S(2)}) copy-start(bf16[128,2048]{1,0:T(8,128)(2,1)} %hid_ref.1) | copy-start | bytes 1572868
